TPU v7x, 512 devices: a whole 4x4x16 slice. The times are simulated.
512 devices in a mesh: fs: 64 (over z, y), tp: 8 (over x, core).
Axes of the slice: x: 4, y: 4, z: 16, core: 2. Of those that a mesh axis runs over, the one named last changes fastest.
Arguments:
- tokens: bfloat16 [49152, 2048], P('fs'), may hold values from -6 to 6
- norm_gain: float32 [2048], replicated, may hold values from 0.1 to 1.9
- gate_weight: bfloat16 [2048, 5120], P('fs', 'tp'), may hold values from -0.125 to 0.125
- up_weight: bfloat16 [2048, 5120], P('fs', 'tp'), may hold values from -0.125 to 0.125
- down_weight: bfloat16 [5120, 2048], P('tp', 'fs'), may hold values from -0.078125 to 0.078125
Outputs:
- mixed: bfloat16 [49152, 2048], P(('fs', 'tp'))
All inputs are finite; a program needn't handle non-finite values.
Results may differ from a plain program's by a relative error of at most 0.014.
Values may be sent and summed in bfloat16 or wider, within the bound.
A program may use at most 64 MiB of HBM per device.

v0:
```python
import jax
import jax.numpy as jnp
from jax import lax
from jax.sharding import Mesh
from jax.sharding import PartitionSpec as P

FS = ("fs_0", "fs_1")
FS_TP = ("fs_0", "fs_1", "tp")


def in_one_piece(arrays, axis, dim, along):
    ends, at = ([], 0)
    for a in arrays[:-1]:
        at += a.shape[along]
        ends.append(at)
    both = jnp.concatenate(arrays, axis=along)
    return tuple(jnp.split(lax.all_gather(both, axis, axis=dim, tiled=True), ends, axis=along))


def whole_of(shard, axes, dim):
    for axis in reversed(axes):
        shard = lax.all_gather(shard, axis, axis=dim, tiled=True)
    return shard


def cut_along(shard, dim, length):
    before, after = (shard.shape[:dim], shard.shape[dim + 1 :])
    return jnp.moveaxis(shard.reshape(*before, length, -1, *after), dim, 0)


def sum_at_owner(shard, axis, dim):
    length = lax.axis_size(axis)
    tiles = lax.all_to_all(cut_along(shard, dim, length), axis, 0, 0, tiled=True)
    return jnp.sum(tiles.astype(jnp.float32), axis=0)


def add_rows(normed, piece):
    return jnp.dot(normed, piece, preferred_element_type=jnp.float32)


def per_device(tokens, norm_gain, gate_weight, up_weight, down_weight):
    values = tokens.astype(jnp.float32)
    scale = lax.rsqrt(jnp.mean(values * values, axis=-1, keepdims=True) + 1e-06)
    normed = (values * scale * norm_gain).astype(jnp.bfloat16)
    pieces = in_one_piece((gate_weight, up_weight), FS, 0, 1)
    gate_proj = add_rows(normed, pieces[0])
    up_proj = add_rows(normed, pieces[1])
    hidden = (jax.nn.silu(gate_proj) * up_proj).astype(jnp.bfloat16)
    down_whole = whole_of(down_weight, FS, 1)
    summed = sum_at_owner(
        jnp.dot(hidden, down_whole, preferred_element_type=jnp.float32).astype(jnp.bfloat16),
        "tp",
        0,
    )
    return summed.astype(jnp.bfloat16)


def solution(mesh):
    split = Mesh(mesh.devices.reshape(16, 4, mesh.shape["tp"]), ("fs_0", "fs_1", "tp"))
    return jax.shard_map(
        per_device,
        mesh=split,
        in_specs=(P(FS, None), P(), P(FS, "tp"), P(FS, "tp"), P("tp", FS)),
        out_specs=P(FS_TP, None),
        check_vma=False,
    )
```

profile of v0, /device:TPU:1, one launch (start us, length us, event | category | flops | bytes accessed | tf_op | source)
XLA Modules:
  0.0 296.5 jit_solution(1876815054470670374)
XLA Ops:
  6.5 0.0 copy-start
  6.5 0.0 copy-start.1
  6.5 0.0 all-gather.3.cloned.1.call-start
  6.5 1.6 pad_maximum_fusion
  8.1 0.0 all-gather.3.cloned.1.call-update
  8.2 0.0 all-gather.5.cloned.1.call-start
  8.2 12.4 %all_gather.10 = bf16[640,128]{0,1:T(8,128)(2,1)} all-gather(bf16[640,32]{0,1:T(8,128)(2,1)} %param.9), channel_id=1, replica_groups=mesh['fs_0'=16,'fs_1'=4,'tp'=8] {'fs_1'}, dimensions={1}, use_global_device_ids=true | all-gather | bytes 204800 | tf_op jit(solution)/shard_map/all_gather | solution.py:22
  20.6 0.0 all-gather.5.cloned.1.call-update
  20.6 2.6 fusion
  23.2 131.9 %all-gather.3.cloned.1.call-done = bf16[2048,1280]{1,0:T(8,128)(2,1)} async-done(((bf16[32,1280]{1,0:T(8,128)(2,1)}), bf16[2048,1280]{1,0:T(8,128)(2,1)}) %all-gather.3.cloned.1.call-update) | async-done | bytes 5242896 | tf_op jit(solution)/shard_map/all_gather | solution.py:17
  155.2 0.0 copy-done
  155.2 0.0 copy-done.1
  155.2 5.7 %fusion.5 = f32[768,640]{1,0:T(8,128)} fusion(bf16[2048,1280]{1,0:T(8,128)(2,1)} %all-gather.3.cloned.1.call-done, bf16[768,2048]{1,0:T(8,128)(2,1)S(1)} %copy-done, f32[2048]{0:T(1024)S(1)} %copy-done.1, f32[768]{0:T(1024)S(1)} %add_rsqrt_fusion), kind=kOutput, calls=%fused_computation.8 | convolution fusion | flops 2019557376 | bytes 7744512 | tf_op jit(solution)/shard_map/dot_general | solution.py:38
  160.9 64.9 %all-gather.5.cloned.1.call-done = bf16[640,2048]{0,1:T(8,128)(2,1)} async-done(((bf16[640,128]{0,1:T(8,128)(2,1)}), bf16[640,2048]{0,1:T(8,128)(2,1)}) %all-gather.5.cloned.1.call-update) | async-done | bytes 2621456 | tf_op jit(solution)/shard_map/all_gather | solution.py:22
  225.8 10.6 %convolution_convert_fusion = bf16[768,2048]{1,0:T(8,128)(2,1)} fusion(bf16[640,2048]{0,1:T(8,128)(2,1)} %all-gather.5.cloned.1.call-done, f32[768,640]{1,0:T(8,128)} %fusion.5, bf16[2048,1280]{1,0:T(8,128)(2,1)} %all-gather.3.cloned.1.call-done, bf16[768,2048]{1,0:T(8,128)(2,1)S(1)} %copy-done, f32[2048]{0:T(1024)S(1)} %copy-done.1, f32[768]{0:T(1024)S(1)} %add_rsqrt_fusion), kind=kOutput, calls=%fused_computation.5 | convolution fusion | flops 4037345280 | bytes 13511680 | tf_op jit(solution)/shard_map/dot_general | solution.py:51
  236.4 51.8 %all_to_all.5 = bf16[8,96,2048]{2,1,0:T(8,128)(2,1)S(1)} all-to-all(bf16[8,96,2048]{2,1,0:T(8,128)(2,1)} %bitcast.2), channel_id=1, replica_groups=mesh['fs_0'=16,'fs_1'=4,'tp'=8] {'tp'}, dimensions={0} | all-to-all | bytes 6291456 | tf_op jit(solution)/shard_map/all_to_all | solution.py:33
  288.2 1.4 reduce_sum.22
  (1 shorter events, 0.0 us)
Async XLA Ops:
  6.5 148.6 %copy-start = (bf16[768,2048]{1,0:T(8,128)(2,1)S(1)}, bf16[768,2048]{1,0:T(8,128)(2,1)}, u32[]{:S(2)}) copy-start(bf16[768,2048]{1,0:T(8,128)(2,1)} %param.5) | copy-start | bytes 9437188
  6.5 148.6 %copy-start.1 = (f32[2048]{0:T(1024)S(1)}, f32[2048]{0:T(1024)}, u32[]{:S(2)}) copy-start(f32[2048]{0:T(1024)} %param.6) | copy-start | bytes 24580
  6.5 148.6 %all-gather.3.cloned.1.call-start = ((), (), s32[]{:S(2)}) async-start(), calls=%async_computation.1 | async-start | bytes 5324800 | tf_op jit(solution)/shard_map/all_gather | solution.py:17
  8.2 217.6 %all-gather.5.cloned.1.call-start = ((), (), s32[]{:S(2)}) async-start(), calls=%async_computation.2 | async-start | bytes 2785280 | tf_op jit(solution)/shard_map/all_gather | solution.py:22
Sparse Core Ops, SparseCore 0:
  10.3 144.8 all-gather.2
  157.2 68.4 all-gather.4
where the time goes:
time: 297 us; the launch traced here: 296 us
  waiting for transfers between devices  197 us (66%)
  blocking collectives  64.2 us (22%)
  matrix products  16.3 us (5%)
  between operations  13.4 us (5%)
  other arithmetic  5.57 us (2%)
    all_gather x1, waiting for transfers between devices, in_one_piece(): lax.all_gather(both, axis, axis=dim, tiled=True)  132 us
    all_gather x1, waiting for transfers between devices, whole_of(): shard = lax.all_gather(shard, axis, axis=dim, tiled=True)  64.9 us
    all_to_all x1, blocking collectives, sum_at_owner(): lax.all_to_all(cut_along(shard, dim, length), axis, 0, 0, tiled=True)  51.8 us
    all_gather x1, blocking collectives, whole_of(): shard = lax.all_gather(shard, axis, axis=dim, tiled=True)  12.4 us
    dot_general x1, matrix products, per_device(): jnp.dot(hidden, down_whole, preferred_element_type=jnp.float32)  10.6 us
  transfers between devices with their start and end apart: 2, of which 2 were waited for; matrix products, arithmetic and copies ran while one was open for 3% of the time, Pallas kernels for 0%

commit v1 on v0

v1 whole, which is shorter than its diff:
```python
import functools

import jax
import jax.numpy as jnp
from jax import lax
from jax.experimental import pallas as pl
from jax.experimental.pallas import tpu as pltpu
from jax.sharding import PartitionSpec as P

MESH = pl.DeviceIdType.MESH
NX, NY = 4, 4
PF = 256
LAG = 8
DIRS = (0, 1)
OFFSETS = (0, -1, 1, 2)


def kernel(nz, tok, gain, gate, up, down, out, tokv, gainv, nc, wq, wp, dq, dp, accq, accp, hid, own, dsend, drecv, xsend,
           xrecv, outb, ld, tokld, outs, d2s, d2r, xs, xr, *sems):
    fs, tp = lax.axis_index("fs"), lax.axis_index("tp")
    z, y = fs // NY, lax.rem(fs, NY)
    x, c = tp // 2, lax.rem(tp, 2)
    rows = tokv.shape[1]
    shard = gate.shape[0]
    half = shard // 2
    plane = shard * NY
    last = nz // 2
    part = NX * rows

    def zdev(d):
        return (lax.rem(z + d + nz, nz) * NY + y, tp)

    def ydev(d):
        return (z * NY + lax.rem(y + d + NY, NY), tp)

    def ypos(d):
        return lax.rem(y + d + NY, NY)

    def xdev(d):
        return (fs, lax.rem(x + d, NX) * 2 + c)

    partner = (fs, x * 2 + 1 - c)

    def remote(src, dst, ss, rs, dev):
        return pltpu.make_async_remote_copy(src_ref=src, dst_ref=dst, send_sem=ss, recv_sem=rs, device_id=dev,
                                            device_id_type=MESH)

    class Gather:
        def __init__(self, q, p, sems):
            self.q, self.p = q, p
            (self.qzs, self.qzr, self.qys, self.qyr, self.qws, self.qwr, self.pzs, self.pzr, self.pys, self.pyr, self.pws,
             self.pwr) = sems

        def at(self, ref, pair, side, yy, h=None):
            start = side * plane + yy * shard
            if h is None:
                return ref.at[pair, pl.ds(pl.multiple_of(start, half), shard), :]
            return ref.at[pair, pl.ds(pl.multiple_of(start + h * half, half), half), :]

        def q_send(self, s, d):
            pair, side = (0, 0) if isinstance(s, int) and s == 0 else (s, d)
            n = 2 * (s + 1) + d
            return remote(self.at(self.q, pair, side, y), self.at(self.q, s + 1, d, y), self.qzs.at[n], self.qzr.at[n],
                          zdev(1 - 2 * d))

        def q_send_last(self, d):
            return remote(self.at(self.q, last - 1, d, y, d), self.at(self.q, 0, 1, y, d), self.qzs.at[d], self.qzr.at[d],
                          zdev(1 - 2 * d))

        def y_send(self, ref, ss, rs, pair, side, n, d):
            here = self.at(ref, pair, side, y)
            return remote(here, here, ss.at[n, d], rs.at[n, d], ydev(1 - 2 * d))

        def y_recv(self, ref, ss, rs, pair, side, n, d):
            here = self.at(ref, pair, side, ypos(2 * d - 1))
            return remote(here, here, ss.at[n, d], rs.at[n, d], ydev(1 - 2 * d))

        def w_send(self, ref, ss, rs, pair, side, n, d):
            here = self.at(ref, pair, side, ypos(2 * d - 1), d)
            return remote(here, here, ss.at[n, d], rs.at[n, d], ydev(1 - 2 * d))

        def w_recv(self, ref, ss, rs, pair, side, n, d):
            here = self.at(ref, pair, side, ypos(2), d)
            return remote(here, here, ss.at[n, d], rs.at[n, d], ydev(1 - 2 * d))

        def q_y1(self, pair, side):
            for d in DIRS:
                self.y_send(self.q, self.qys, self.qyr, pair, side, 2 * pair + side, d).start()

        def q_y2(self, pair, side):
            for d in DIRS:
                self.y_recv(self.q, self.qys, self.qyr, pair, side, 2 * pair + side, d).wait_recv()
                self.w_send(self.q, self.qws, self.qwr, pair, side, 2 * pair + side, d).start()

        def q_y3(self, pair, side):
            for d in DIRS:
                self.w_recv(self.q, self.qws, self.qwr, pair, side, 2 * pair + side, d).wait_recv()

        def p_send(self, s, d, j):
            pair, side = (0, 0) if isinstance(s, int) and s == 0 else (s, d)
            yy = ypos(OFFSETS[j])
            n = 2 * (s + 1) + d
            return remote(self.at(self.p, pair, side, yy), self.at(self.p, s + 1, d, yy), self.pzs.at[n, j],
                          self.pzr.at[n, j], zdev(1 - 2 * d))

        def p_send_last(self, d, j):
            yy = ypos(OFFSETS[j])
            return remote(self.at(self.p, last - 1, d, yy), self.at(self.p, 0, 1, yy), self.pzs.at[1, j], self.pzr.at[1, j],
                          zdev(1 - 2 * d))

        def begin_q(self):
            for d in DIRS:
                self.q_send(0, d).start()
            self.q_y1(0, 0)

        def begin_p(self):
            for d in DIRS:
                self.y_send(self.p, self.pys, self.pyr, 0, 0, 0, d).start()
            for d in DIRS:
                self.p_send(0, d, 0).start()

        def begin_p2(self):
            for d in DIRS:
                self.y_recv(self.p, self.pys, self.pyr, 0, 0, 0, d).wait_recv()
                self.w_send(self.p, self.pws, self.pwr, 0, 0, 0, d).start()
                for e in DIRS:
                    self.p_send(0, e, 1 + d).start()

        def begin_p3(self):
            for d in DIRS:
                self.w_recv(self.p, self.pws, self.pwr, 0, 0, 0, d).wait_recv()
            for d in DIRS:
                self.p_send(0, d, 3).start()

        def step_q(self, s):
            @pl.when(s < last)
            def _():
                for d in DIRS:
                    self.q_send(s - 1, d).wait_recv()

                    @pl.when(s < last - 1)
                    def _():
                        self.q_send(s, d).start()

                    @pl.when(s == last - 1)
                    def _():
                        self.q_send_last(d).start()

                for d in DIRS:
                    self.q_y1(s, d)

            @pl.when(s == last)
            def _():
                for d in DIRS:
                    self.q_send_last(d).wait_recv()
                self.q_y1(0, 1)

        def step_p(self, s, j):
            @pl.when(s < last)
            def _():
                for d in DIRS:
                    self.p_send(s - 1, d, j).wait_recv()

                    @pl.when(s < last - 1)
                    def _():
                        self.p_send(s, d, j).start()

                    if d == j // 2:

                        @pl.when(s == last - 1)
                        def _():
                            self.p_send_last(d, j).start()

            @pl.when(s == last)
            def _():
                self.p_send_last(j // 2, j).wait_recv()

        def each_slot(self, s, act):
            @pl.when(s == 0)
            def _():
                act(0, 0)

            @pl.when(jnp.logical_and(s > 0, s < last))
            def _():
                act(s, 0)
                act(s, 1)

            @pl.when(s == last)
            def _():
                act(0, 1)

        def finish(self):
            def one(n, _):
                for d in DIRS:
                    self.y_send(self.q, self.qys, self.qyr, n // 2, lax.rem(n, 2), n, d).wait_send()
                    self.w_send(self.q, self.qws, self.qwr, n // 2, lax.rem(n, 2), n, d).wait_send()

                return 0

            lax.fori_loop(0, nz, one, 0)
            for d in DIRS:
                self.q_send_last(d).wait_send()
                self.y_send(self.p, self.pys, self.pyr, 0, 0, 0, d).wait_send()
                self.w_send(self.p, self.pws, self.pwr, 0, 0, 0, d).wait_send()
            for j in range(NY):
                self.p_send_last(j // 2, j).wait_send()

            def two(s, _):
                for d in DIRS:
                    self.q_send(s, d).wait_send()
                    for j in range(NY):
                        self.p_send(s, d, j).wait_send()
                return 0

            lax.fori_loop(0, last - 1, two, 0)

    first = Gather(wq, wp, sems[:12])
    second = Gather(dq, dp, sems[12:])

    unit = gate.shape[1]
    mine = pl.ds(pl.multiple_of(y * shard, shard), shard)
    qf = unit - PF
    loads = [
        (gate.at[:, pl.ds(PF, qf)], wq.at[0, mine, pl.ds(0, qf)]),
        (up.at[:, pl.ds(PF, qf)], wq.at[0, mine, pl.ds(qf, qf)]),
        (gate.at[:, pl.ds(0, PF)], wp.at[0, mine, pl.ds(0, PF)]),
        (up.at[:, pl.ds(0, PF)], wp.at[0, mine, pl.ds(PF, PF)]),
        (down.at[:, pl.ds(PF, qf)], dq.at[0, mine, :]),
        (down.at[:, pl.ds(0, PF)], dp.at[0, mine, :]),
        (gain, gainv),
    ]
    loads = [pltpu.make_async_copy(a, b, ld.at[i]) for i, (a, b) in enumerate(loads)]
    for copy in loads:
        copy.start()
    barrier = pltpu.get_barrier_semaphore()
    peers = [zdev(1), zdev(-1), ydev(1), ydev(-1), partner] + [xdev(d) for d in range(1, NX)]
    for dev in peers:
        pl.semaphore_signal(barrier, inc=1, device_id=dev, device_id_type=MESH)
    tok_loads = []
    for i in range(2 * NX):
        core = c if i < NX else 1 - c
        owner = lax.rem(x + i % NX, NX) * 2 + core
        tok_loads.append(pltpu.make_async_copy(tok.at[pl.ds(pl.multiple_of(owner * rows, 32), rows), :], tokv.at[i], tokld.at[i]))
        tok_loads[-1].start()
    pl.semaphore_wait(barrier, len(peers))

    loads[0].wait()
    loads[1].wait()
    first.begin_q()
    loads[2].wait()
    loads[3].wait()
    first.begin_p()
    for copy in loads[4:]:
        copy.wait()
    for copy in tok_loads:
        copy.wait()
    first.begin_p2()

    sub = 32

    def norm(i):
        def some(r, _):
            at = pl.ds(pl.multiple_of(r * sub, sub), sub)
            to = pl.ds(pl.multiple_of(i * rows + r * sub, sub), sub)
            values = tokv[i, at, :].astype(jnp.float32)
            scale = lax.rsqrt(jnp.mean(values * values, axis=-1, keepdims=True) + 1e-6)
            normed = (values * scale * gainv[...]).astype(jnp.bfloat16)
            for k in range(nz):
                nc[k, to, :] = normed[:, k * plane:(k + 1) * plane]
            return 0

        lax.fori_loop(0, rows // sub, some, 0)
        at = pl.ds(pl.multiple_of(i * rows, sub), rows)
        accq[at, :] = jnp.zeros((rows, 2 * qf), jnp.float32)
        accp[at, :] = jnp.zeros((rows, 2 * PF), jnp.float32)

    block = part // 2

    def project(s, j):
        at = pl.ds(j * block, block)
        za = lax.rem(z - lax.rem(s, last) + nz, nz)
        zb = lax.rem(z + s, nz)
        left = jnp.concatenate([nc[za, at, :], nc[zb, at, :]], axis=1)
        pair = lax.rem(s, last)
        accq[at, :] += jnp.dot(left, wq[pair], preferred_element_type=jnp.float32)
        accp[at, :] += jnp.dot(left, wp[pair], preferred_element_type=jnp.float32)

    def gated(j):
        at = pl.ds(j * block, block)
        g, u = accp[at, :PF], accp[at, PF:]
        hid[at, :PF] = (g / (1.0 + jnp.exp(-g)) * u).astype(jnp.bfloat16)
        g, u = accq[at, :qf], accq[at, qf:]
        hid[at, PF:] = (g / (1.0 + jnp.exp(-g)) * u).astype(jnp.bfloat16)

    def dot_t(a, b):
        return lax.dot_general(a, b, (((1,), (1,)), ((), ())), preferred_element_type=jnp.float32)

    def to_partner(pair):
        return remote(dsend.at[pair], drecv.at[pair], d2s.at[pair], d2r.at[pair], partner)

    def to_owner(pair, d):
        return remote(xsend.at[pair, d - 1], xrecv.at[pair, d - 1], xs.at[pair, d - 1], xr.at[pair, d - 1], xdev(d))

    def to_out(s, side):
        pair = lax.rem(s, last)
        zz = lax.rem(z + s, nz) if side else lax.rem(z - pair + nz, nz)
        return pltpu.make_async_copy(outb.at[pair, :, pl.ds(side * plane, plane)],
                                     out.at[:, pl.ds(pl.multiple_of(zz * plane, plane), plane)], outs.at[pair, side])

    def mix(s):
        pair = lax.rem(s, last)
        for j in (2, 3, 0, 1):
            at = pl.ds(j * block, block)
            here = dot_t(hid[at, :PF], dp[pair]) + dot_t(hid[at, PF:], dq[pair])
            if j >= 2:
                dsend[pair, pl.ds((j - 2) * block, block), :] = here.astype(jnp.bfloat16)
                if j == 3:
                    to_partner(pair).start()
            else:
                own[pair, at, :] = here

    def chip_sum(s):
        pair = lax.rem(s, last)
        to_partner(pair).wait_recv()
        for d in (2, 1, 3, 0):
            at = pl.ds(d * rows, rows)
            both = own[pair, at, :] + drecv[pair, at, :].astype(jnp.float32)
            if d:
                xsend[pair, d - 1] = both.astype(jnp.bfloat16)
            else:
                own[pair, at, :] = both
        for d in (2, 1, 3):
            to_owner(pair, d).start()

    def total(s):
        pair = lax.rem(s, last)
        both = own[pair, pl.ds(0, rows), :]
        for d in range(1, NX):
            to_owner(pair, d).wait_recv()
            both += xrecv[pair, d - 1].astype(jnp.float32)
        outb[pair] = both.astype(jnp.bfloat16)
        for side in DIRS:
            to_out(s, side).start()

    def compute(t, j):
        if j == 0:
            first.each_slot(t - 2, first.q_y3)

        @pl.when(t <= 2)
        def _():
            norm((t - 1) * 4 + j)

        @pl.when(jnp.logical_and(t >= 3, t <= last + 2))
        def _():
            project(t - 2, j)

        @pl.when(t == last + 2)
        def _():
            gated(j)

    def inside(v):
        return jnp.logical_and(v >= 1, v <= last)

    def body(t, _):
        d = t - LAG

        @pl.when(t <= last)
        def _():
            first.step_q(t)

        for j in range(NY):
            @pl.when(t <= last)
            def _():
                first.step_p(t, j)

            if j == 0:
                @pl.when(t == 1)
                def _():
                    first.begin_p3()

                first.each_slot(t - 1, first.q_y2)

            @pl.when(t <= last + 2)
            def _():
                compute(t, j)

        @pl.when(d == 0)
        def _():
            second.begin_q()
            second.begin_p()

        @pl.when(inside(d))
        def _():
            second.step_q(d)

        @pl.when(d == 1)
        def _():
            second.begin_p2()
            second.begin_p3()

        second.each_slot(d - 1, second.q_y2)

        u = t - last - 2

        @pl.when(inside(u - 1))
        def _():
            chip_sum(u - 1)

        for j in range(2):
            @pl.when(inside(d))
            def _():
                second.step_p(d, j)

        @pl.when(inside(u))
        def _():
            @pl.when(u == 1)
            def _():
                second.each_slot(0, second.q_y3)

            second.each_slot(u, second.q_y3)
            mix(u)

        for j in range(2, 4):
            @pl.when(inside(d))
            def _():
                second.step_p(d, j)

        @pl.when(inside(u - 3))
        def _():
            total(u - 3)

        return 0

    lax.fori_loop(1, 2 * last + 6, body, 0)

    first.finish()
    second.finish()

    def done(s, _):
        pair = lax.rem(s, last)
        to_partner(pair).wait_send()
        for d in range(1, NX):
            to_owner(pair, d).wait_send()
        for side in DIRS:
            to_out(s, side).wait()
        return 0

    lax.fori_loop(1, last + 1, done, 0)


def solution(mesh):
    nz = mesh.shape["fs"] // NY

    def per_device(tokens, norm_gain, gate, up, down):
        m, width = tokens.shape
        shard, unit = gate.shape
        rows = m // (2 * NX)
        part = NX * rows
        qf = unit - PF
        pairs = nz // 2
        deep = 2 * NY * shard
        bf, f32, dma = jnp.bfloat16, jnp.float32, pltpu.SemaphoreType.DMA
        gather_sems = [dma((nz,)), dma((nz,))] + [dma((nz, 2))] * 4 + [dma((nz, NY))] * 2 + [dma((1, 2))] * 4
        return pl.pallas_call(
            functools.partial(kernel, nz),
            out_shape=jax.ShapeDtypeStruct((rows, width), bf),
            in_specs=[pl.BlockSpec(memory_space=pltpu.HBM)] * 5,
            out_specs=pl.BlockSpec(memory_space=pltpu.HBM),
            scratch_shapes=[
                pltpu.VMEM((2 * NX, rows, width), bf),
                pltpu.VMEM((1, width), f32),
                pltpu.VMEM((nz, m, NY * shard), bf),
                pltpu.VMEM((pairs, deep, 2 * qf), bf),
                pltpu.VMEM((pairs, deep, 2 * PF), bf),
                pltpu.VMEM((pairs, deep, qf), bf),
                pltpu.VMEM((pairs, deep, PF), bf),
                pltpu.VMEM((m, 2 * qf), f32),
                pltpu.VMEM((m, 2 * PF), f32),
                pltpu.VMEM((m, unit), bf),
                pltpu.VMEM((pairs, part, deep), f32),
                pltpu.VMEM((pairs, part, deep), bf),
                pltpu.VMEM((pairs, part, deep), bf),
                pltpu.VMEM((pairs, NX - 1, rows, deep), bf),
                pltpu.VMEM((pairs, NX - 1, rows, deep), bf),
                pltpu.VMEM((pairs, rows, deep), bf),
                dma((7,)),
                dma((2 * NX,)),
                dma((pairs, 2)),
                dma((pairs,)),
                dma((pairs,)),
                dma((pairs, NX - 1)),
                dma((pairs, NX - 1)),
            ]
            + gather_sems * 2,
            compiler_params=pltpu.CompilerParams(collective_id=0, has_side_effects=True, vmem_limit_bytes=60 * 1024 * 1024),
        )(tokens, norm_gain.reshape(1, width), gate, up, down.T)

    return jax.shard_map(
        per_device,
        mesh=mesh,
        in_specs=(P("fs", None), P(), P("fs", "tp"), P("fs", "tp"), P("tp", "fs")),
        out_specs=P(("fs", "tp"), None),
        check_vma=False,
    )
```

time: 297 us -> 105 us (0.35)
  waiting for transfers between devices: 197 us -> 0 us
  Pallas kernels: 0 us -> 103 us
  blocking collectives: 64.2 us -> 0 us
  matrix products: 16.3 us -> 0 us
  between operations: 13.4 us -> 0.01 us
  other arithmetic: 5.57 us -> 0 us
    all_gather x2 -> x0, waiting for transfers between devices: 197 us -> none  [the longest x1 132 us: in_one_piece(): lax.all_gather(both, axis, axis=dim, tiled=True)]
    pallas_call x0 -> x1, Pallas kernels: none -> 103 us  [per_device(): pl.pallas_call(functools.partial(kernel, nz), out_shape=jax.ShapeDtypeStr...]
    all_to_all x1 -> x0, blocking collectives: 51.8 us -> none  [sum_at_owner(): lax.all_to_all(cut_along(shard, dim, length), axis, 0, 0, tiled=True)]
    dot_general x2 -> x0, matrix products: 16.3 us -> none  [the longest x1 10.6 us: per_device(): jnp.dot(hidden, down_whole, preferred_element_type=jnp.float32)]
    all_gather x1 -> x0, blocking collectives: 12.4 us -> none  [whole_of(): shard = lax.all_gather(shard, axis, axis=dim, tiled=True)]
    reduce_sum x2 -> x0, other arithmetic: 3.97 us -> none  [the longest x1 2.57 us: per_device(): scale = lax.rsqrt(jnp.mean(values * values, axis=-1, keepdims=True) + 1e-06)]
  transfers between devices with their start and end apart: 2 -> 0, of which waited for: 2 -> 0; matrix products, arithmetic and copies ran while one was open for 3% -> 0% of each run, Pallas kernels for 0% -> 0%
where the time goes in v1:
time: 105 us
  Pallas kernels  103 us (98%)
  local copies, waits for them, and re-layouts  1.77 us (2%)
    pallas_call x1, Pallas kernels, per_device(): pl.pallas_call(functools.partial(kernel, nz), out_shape=jax.ShapeDtypeStr...  103 us

profile of v1, /device:TPU:1, one launch (start us, length us, event | category | flops | bytes accessed | tf_op | source)
XLA Modules:
  0.0 105.2 jit_solution(16943086676605522746)
XLA Ops:
  0.0 103.4 %shard_map.55 = bf16[96,2048]{1,0:T(8,128)(2,1)} custom-call(bf16[768,2048]{1,0:T(8,128)(2,1)} %tok.1, f32[1,2048]{1,0:T(1,128)} %bitcast.3, bf16[32,640]{1,0:T(8,128)(2,1)} %gate.1, bf16[32,640]{1,0:T(8,128)(2,1)} %up.1, bf16[32,640]{1,0:T(8,128)(2,1)} %bitcast.2), custom_call_target="tpu_custom_call" | custom-call | tf_op jit(solution)/shard_map/pallas_call | solution.py:464
  103.4 1.8 %copy.7 = bf16[96,2048]{1,0:T(8,128)(2,1)} copy(bf16[96,2048]{1,0:T(8,128)(2,1)} %shard_map.55) | data formatting | bytes 786432

commit v2 on v1

v2 whole, which is shorter than its diff:
```python
import functools

import jax
import jax.numpy as jnp
from jax import lax
from jax.experimental import pallas as pl
from jax.experimental.pallas import tpu as pltpu
from jax.sharding import PartitionSpec as P

MESH = pl.DeviceIdType.MESH
NX, NY = 4, 4
PF = 256
LAG = 8
MIX = 3
DIRS = (0, 1)
OFFSETS = (0, -1, 1, 2)
RING = 4


def kernel(nz, tok, gain, gate, up, down, out, tokv, gainv, nc, wq, wp, dq, dp, accq, accp, hid, own, dsend, drecv, xsend,
           xrecv, outb, ld, outs, d2s, d2r, xs, xr, *sems):
    fs, tp = lax.axis_index("fs"), lax.axis_index("tp")
    z, y = fs // NY, lax.rem(fs, NY)
    x, c = tp // 2, lax.rem(tp, 2)
    rows = tokv.shape[1]
    shard = gate.shape[0]
    half = shard // 2
    plane = shard * NY
    last = nz // 2
    part = NX * rows
    scope = jax.named_scope

    def zdev(d):
        return (lax.rem(z + d + nz, nz) * NY + y, tp)

    def ydev(d):
        return (z * NY + lax.rem(y + d + NY, NY), tp)

    def ypos(d):
        return lax.rem(y + d + NY, NY)

    def xdev(d):
        return (fs, lax.rem(x + d, NX) * 2 + c)

    partner = (fs, x * 2 + 1 - c)

    def remote(src, dst, ss, rs, dev):
        return pltpu.make_async_remote_copy(src_ref=src, dst_ref=dst, send_sem=ss, recv_sem=rs, device_id=dev,
                                            device_id_type=MESH)

    class Gather:
        def __init__(self, q, p, sems):
            self.q, self.p = q, p
            (self.qzs, self.qzr, self.qls, self.qlr, self.pzs, self.pzr, self.pls, self.plr, self.yes, self.yer, self.yds,
             self.ydr) = sems

        def at(self, ref, pair, side, yy, h=None):
            start, size = yy * shard + (0 if h is None else h * half), shard if h is None else half
            if side is None:
                return ref.at[pair, :, pl.ds(pl.multiple_of(start, half), size), :]
            return ref.at[pair, side, pl.ds(pl.multiple_of(start, half), size), :]

        def q_send(self, s, d):
            pair, side = (0, 0) if isinstance(s, int) and s == 0 else (s, d)
            n = lax.rem(s + 1, RING)
            return remote(self.at(self.q, pair, side, y), self.at(self.q, s + 1, d, y), self.qzs.at[d], self.qzr.at[n, d],
                          zdev(1 - 2 * d))

        def q_last(self, d):
            return remote(self.at(self.q, last - 1, d, y, d), self.at(self.q, 0, 1, y, d), self.qls.at[d], self.qlr.at[d],
                          zdev(1 - 2 * d))

        def where(self, kind):
            if isinstance(kind, int):
                ref, pair, side = ((self.q, 0, 0), (self.q, 0, 1), (self.p, 0, 0))[kind]
                return ref, pair, side, self.yes, self.yer, kind
            return self.q, kind, None, self.yds, self.ydr, kind

        def y_sem(self, kind, ss, rs, hop, d):
            if isinstance(kind, int):
                return ss.at[kind, hop, d], rs.at[kind, hop, d]
            return ss.at[hop, d], rs.at[kind - 1, hop, d]

        def y_send(self, kind, d):
            ref, pair, side, ss, rs, n = self.where(kind)
            here = self.at(ref, pair, side, y)
            return remote(here, here, *self.y_sem(kind, ss, rs, 0, d), ydev(1 - 2 * d))

        def y_recv(self, kind, d):
            ref, pair, side, ss, rs, n = self.where(kind)
            here = self.at(ref, pair, side, ypos(2 * d - 1))
            return remote(here, here, *self.y_sem(kind, ss, rs, 0, d), ydev(1 - 2 * d))

        def w_send(self, kind, d):
            ref, pair, side, ss, rs, n = self.where(kind)
            here = self.at(ref, pair, side, ypos(2 * d - 1), d)
            return remote(here, here, *self.y_sem(kind, ss, rs, 1, d), ydev(1 - 2 * d))

        def w_recv(self, kind, d):
            ref, pair, side, ss, rs, n = self.where(kind)
            here = self.at(ref, pair, side, ypos(2), d)
            return remote(here, here, *self.y_sem(kind, ss, rs, 1, d), ydev(1 - 2 * d))

        def y1(self, kind):
            for d in DIRS:
                if not isinstance(kind, int):

                    @pl.when(kind > 1)
                    def _():
                        self.y_send(kind - 1, d).wait_send()

                self.y_send(kind, d).start()

        def y2(self, kind):
            for d in DIRS:
                self.y_recv(kind, d).wait_recv()
                if not isinstance(kind, int):

                    @pl.when(kind > 1)
                    def _():
                        self.w_send(kind - 1, d).wait_send()

                self.w_send(kind, d).start()

        def y3(self, kind):
            for d in DIRS:
                self.w_recv(kind, d).wait_recv()

        def at_step(self, s, act):
            @pl.when(s == 0)
            def _():
                act(0)

            @pl.when(jnp.logical_and(s > 0, s < last))
            def _():
                act(s)

            @pl.when(s == last)
            def _():
                act(1)

        def p_send(self, s, d, j):
            pair, side = (0, 0) if isinstance(s, int) and s == 0 else (s, d)
            yy = ypos(OFFSETS[j])
            n = lax.rem(s + 1, RING)
            return remote(self.at(self.p, pair, side, yy), self.at(self.p, s + 1, d, yy), self.pzs.at[d, j],
                          self.pzr.at[n, d, j], zdev(1 - 2 * d))

        def p_last(self, d, j):
            yy = ypos(OFFSETS[j])
            return remote(self.at(self.p, last - 1, d, yy), self.at(self.p, 0, 1, yy), self.pls.at[j], self.plr.at[j],
                          zdev(1 - 2 * d))

        def begin_q(self):
            for d in DIRS:
                self.q_send(0, d).start()

        def begin_p(self, j):
            for d in DIRS:
                self.p_send(0, d, j).start()

        def step_q(self, s):
            @pl.when(s < last)
            def _():
                for d in DIRS:
                    self.q_send(s - 1, d).wait_recv()

                    @pl.when(s < last - 1)
                    def _():
                        self.q_send(s - 1, d).wait_send()
                        self.q_send(s, d).start()

                    @pl.when(s == last - 1)
                    def _():
                        self.q_last(d).start()

                self.y1(s)

            @pl.when(s == last)
            def _():
                for d in DIRS:
                    self.q_last(d).wait_recv()
                self.y1(1)

        def step_p(self, s, j):
            @pl.when(s < last)
            def _():
                for d in DIRS:
                    self.p_send(s - 1, d, j).wait_recv()

                    @pl.when(s < last - 1)
                    def _():
                        self.p_send(s - 1, d, j).wait_send()
                        self.p_send(s, d, j).start()

                    if d == j // 2:

                        @pl.when(s == last - 1)
                        def _():
                            self.p_last(d, j).start()

            @pl.when(s == last)
            def _():
                self.p_last(j // 2, j).wait_recv()

        def finish(self):
            for d in DIRS:
                self.q_send(last - 2, d).wait_send()
                self.q_last(d).wait_send()
                for kind in (0, 1, 2, jnp.int32(last - 1)):
                    self.y_send(kind, d).wait_send()
                    self.w_send(kind, d).wait_send()
                for j in range(NY):
                    self.p_send(last - 2, d, j).wait_send()
            for j in range(NY):
                self.p_last(j // 2, j).wait_send()

    first = Gather(wq, wp, sems[:12])
    second = Gather(dq, dp, sems[12:])

    unit = gate.shape[1]
    mine = pl.ds(pl.multiple_of(y * shard, shard), shard)
    qf = unit - PF
    loads = [
        (gate.at[:, pl.ds(0, PF)], wp.at[0, 0, mine, pl.ds(0, PF)]),
        (up.at[:, pl.ds(0, PF)], wp.at[0, 0, mine, pl.ds(PF, PF)]),
        (gate.at[:, pl.ds(PF, qf)], wq.at[0, 0, mine, pl.ds(0, qf)]),
        (up.at[:, pl.ds(PF, qf)], wq.at[0, 0, mine, pl.ds(qf, qf)]),
        (down.at[:, pl.ds(PF, qf)], dq.at[0, 0, mine, :]),
        (down.at[:, pl.ds(0, PF)], dp.at[0, 0, mine, :]),
        (gain, gainv),
    ]
    loads = [pltpu.make_async_copy(a, b, ld.at[i]) for i, (a, b) in enumerate(loads)]
    for copy in loads:
        copy.start()
    barrier = pltpu.get_barrier_semaphore()
    peers = [zdev(1), zdev(-1), ydev(1), ydev(-1), partner] + [xdev(d) for d in range(1, NX)]
    for dev in peers:
        pl.semaphore_signal(barrier, inc=1, device_id=dev, device_id_type=MESH)
    tok_sem = ld.at[len(loads)]
    for i in range(2 * NX):
        core = c if i < NX else 1 - c
        owner = lax.rem(x + i % NX, NX) * 2 + core
        pltpu.make_async_copy(tok.at[pl.ds(pl.multiple_of(owner * rows, 32), rows), :], tokv.at[i], tok_sem).start()
    sub = 32

    def norm(i):
        def some(r, _):
            at = pl.ds(pl.multiple_of(r * sub, sub), sub)
            to = pl.ds(pl.multiple_of(i * rows + r * sub, sub), sub)
            values = tokv[i, at, :].astype(jnp.float32)
            scale = lax.rsqrt(jnp.mean(values * values, axis=-1, keepdims=True) + 1e-6)
            normed = (values * scale * gainv[...]).astype(jnp.bfloat16)
            for k in range(nz):
                nc[k, to, :] = normed[:, k * plane:(k + 1) * plane]
            return 0

        lax.fori_loop(0, rows // sub, some, 0)
        at = pl.ds(pl.multiple_of(i * rows, sub), rows)
        accq[at, :] = jnp.zeros((rows, 2 * qf), jnp.float32)
        accp[at, :] = jnp.zeros((rows, 2 * PF), jnp.float32)

    EARLY = 2

    with scope("barrier"):
        pl.semaphore_wait(barrier, len(peers))
    with scope("b1"):
        loads[0].wait()
        loads[1].wait()
        first.y1(2)
        first.begin_p(0)
        loads[2].wait()
        loads[3].wait()
        first.begin_q()
    with scope("b2"):
        for copy in loads[4:]:
            copy.wait()
        pltpu.make_async_copy(tokv, tokv, tok_sem).wait()
        for i in range(EARLY):
            norm(i)
    with scope("b3"):
        first.y2(2)
        first.begin_p(1)
        first.begin_p(2)
        first.y1(0)

    block = part // 2

    def project(s, j):
        at = pl.ds(j * block, block)
        pair = lax.rem(s, last)
        za, zb = lax.rem(z - pair + nz, nz), lax.rem(z + s, nz)
        left = jnp.concatenate([nc[za, at, :], nc[zb, at, :]], axis=1)
        accq[at, :] += jnp.dot(left, wq[pair].reshape(2 * plane, 2 * qf), preferred_element_type=jnp.float32)
        accp[at, :] += jnp.dot(left, wp[pair].reshape(2 * plane, 2 * PF), preferred_element_type=jnp.float32)

    def gated(j):
        at = pl.ds(j * block, block)
        g, u = accp[at, :PF], accp[at, PF:]
        hid[at, :PF] = (g / (1.0 + jnp.exp(-g)) * u).astype(jnp.bfloat16)
        g, u = accq[at, :qf], accq[at, qf:]
        hid[at, PF:] = (g / (1.0 + jnp.exp(-g)) * u).astype(jnp.bfloat16)

    def dot_t(a, b):
        return lax.dot_general(a, b, (((1,), (1,)), ((), ())), preferred_element_type=jnp.float32)

    class Columns:
        def __init__(self, s, side):
            self.s = s
            self.pair = 0 if side is not None else s
            self.sides = DIRS if side is None else (side,)
            self.cols = pl.ds(self.sides[0] * plane, plane * len(self.sides))

        def to_partner(self):
            return remote(dsend.at[self.pair, :, self.cols], drecv.at[self.pair, :, self.cols], d2s.at[self.s], d2r.at[self.s],
                          partner)

        def to_owner(self, d):
            return remote(xsend.at[self.pair, d - 1, :, self.cols], xrecv.at[self.pair, d - 1, :, self.cols],
                          xs.at[self.s, d - 1], xr.at[self.s, d - 1], xdev(d))

        def to_out(self, side):
            zz = lax.rem(z + self.s, nz) if side else lax.rem(z - self.pair + nz, nz)
            return pltpu.make_async_copy(outb.at[self.pair, :, pl.ds(side * plane, plane)],
                                         out.at[:, pl.ds(pl.multiple_of(zz * plane, plane), plane)],
                                         outs.at[self.pair, side])

        def mix(self, blocks):
            n = len(self.sides)
            if n == 2:
                bp, bq = dp[self.pair].reshape(2 * plane, PF), dq[self.pair].reshape(2 * plane, qf)
            else:
                bp, bq = dp[0, self.sides[0]], dq[0, self.sides[0]]
            for j in blocks:
                at = pl.ds(j * block, block)
                here = dot_t(hid[at, :PF], bp) + dot_t(hid[at, PF:], bq)
                if j >= 2:
                    dsend[self.pair, pl.ds((j - 2) * block, block), self.cols] = here.astype(jnp.bfloat16)
                else:
                    own[self.pair, at, self.cols] = here

        def chip_sum(self):
            self.to_partner().wait_recv()
            for d in (2, 1, 3, 0):
                at = pl.ds(d * rows, rows)
                both = own[self.pair, at, self.cols] + drecv[self.pair, at, self.cols].astype(jnp.float32)
                if d:
                    xsend[self.pair, d - 1, :, self.cols] = both.astype(jnp.bfloat16)
                else:
                    own[self.pair, at, self.cols] = both
            for d in (2, 1, 3):
                self.to_owner(d).start()

        def total(self):
            both = own[self.pair, pl.ds(0, rows), self.cols]
            for d in range(1, NX):
                self.to_owner(d).wait_recv()
                both += xrecv[self.pair, d - 1, :, self.cols].astype(jnp.float32)
            outb[self.pair, :, self.cols] = both.astype(jnp.bfloat16)
            for side in self.sides:
                self.to_out(side).start()

        def finish(self):
            self.to_partner().wait_send()
            for d in range(1, NX):
                self.to_owner(d).wait_send()
            for side in self.sides:
                self.to_out(side).wait()

    def columns(s, act):
        @pl.when(s == 0)
        def _():
            act(Columns(0, 0))

        @pl.when(jnp.logical_and(s > 0, s < last))
        def _():
            act(Columns(s, None))

        @pl.when(s == last)
        def _():
            act(Columns(last, 1))

    def compute(t, j):
        @pl.when(t <= 2)
        def _():
            i = EARLY + (t - 1) * 4 + j

            @pl.when(i < 2 * NX)
            def _():
                norm(i)

        @pl.when(jnp.logical_and(t >= 3, t <= last + 2))
        def _():
            project(t - 2, j)

        @pl.when(t == last + 2)
        def _():
            gated(j)

    def inside(v):
        return jnp.logical_and(v >= 1, v <= last)

    def both(a, b):
        return jnp.logical_and(a, b)

    def body(t, _):
        d = t - LAG
        u = d - MIX

        def when(cond, name, act):
            @pl.when(cond)
            def _():
                with scope(name):
                    act()

        when(t <= last, "q", lambda: first.step_q(t))
        when(t <= last, "p0", lambda: first.step_p(t, 0))

        @pl.when(t == 1)
        def _():
            with scope("y3p"):
                first.y3(2)
                first.begin_p(3)

        when(t <= last, "p1", lambda: first.step_p(t, 1))
        when(t <= last + 1, "y2", lambda: first.at_step(t - 1, first.y2))
        when(t <= last + 2, "y3", lambda: first.at_step(t - 2, first.y3))
        when(t <= last + 2, "c0", lambda: compute(t, 0))
        when(t <= last + 2, "c1", lambda: compute(t, 1))
        when(t <= last, "p2", lambda: first.step_p(t, 2))
        when(t <= last + 2, "c2", lambda: compute(t, 2))
        when(t <= last, "p3", lambda: first.step_p(t, 3))
        when(t <= last + 2, "c3", lambda: compute(t, 3))

        when(t == 2, "e1", lambda: (second.y1(2), second.y1(0)))
        when(t == 4, "e2", lambda: (second.y2(2), second.y2(0)))
        when(t == 6, "e3", lambda: (second.y3(2), second.y3(0)))

        @pl.when(d == 0)
        def _():
            second.begin_q()
            for j in range(NY):
                second.begin_p(j)

        when(inside(d), "dq", lambda: second.step_q(d))
        when(both(u >= 1, u <= last + 1), "chip", lambda: columns(u - 1, Columns.chip_sum))
        when(inside(d), "dp0", lambda: second.step_p(d, 0))
        when(both(u >= 1, u <= last), "dy3", lambda: second.at_step(u, second.y3))

        @pl.when(both(u >= 0, u <= last))
        def _():
            with scope("mixa"):
                columns(u, lambda k: (k.mix((2, 3)), k.to_partner().start()))

        when(inside(d), "dp1", lambda: second.step_p(d, 1))

        @pl.when(both(u >= 0, u <= last))
        def _():
            with scope("mixb"):
                columns(u, lambda k: k.mix((0, 1)))

        when(inside(d), "dp2", lambda: second.step_p(d, 2))
        when(inside(d), "dp3", lambda: second.step_p(d, 3))
        when(inside(d - 1), "dy2", lambda: second.at_step(d - 1, second.y2))
        when(both(u >= 3, u <= last + 3), "total", lambda: columns(u - 3, Columns.total))
        return 0

    lax.fori_loop(1, last + LAG + MIX + 4, body, 0)

    with scope("finish"):
        first.finish()
        second.finish()

        def done(s, _):
            columns(s, Columns.finish)
            return 0

        lax.fori_loop(0, last + 1, done, 0)


def solution(mesh):
    nz = mesh.shape["fs"] // NY

    def per_device(tokens, norm_gain, gate, up, down):
        m, width = tokens.shape
        shard, unit = gate.shape
        rows = m // (2 * NX)
        part = NX * rows
        qf = unit - PF
        pairs = nz // 2
        plane = NY * shard
        deep = 2 * plane
        bf, f32, dma = jnp.bfloat16, jnp.float32, pltpu.SemaphoreType.DMA
        gather_sems = [
            dma((2,)), dma((RING, 2)), dma((2,)), dma((2,)),
            dma((2, NY)), dma((RING, 2, NY)), dma((NY,)), dma((NY,)),
            dma((3, 2, 2)), dma((3, 2, 2)), dma((2, 2)), dma((pairs - 1, 2, 2)),
        ]
        return pl.pallas_call(
            functools.partial(kernel, nz),
            out_shape=jax.ShapeDtypeStruct((rows, width), bf),
            in_specs=[pl.BlockSpec(memory_space=pltpu.HBM)] * 5,
            out_specs=pl.BlockSpec(memory_space=pltpu.HBM),
            scratch_shapes=[
                pltpu.VMEM((2 * NX, rows, width), bf),
                pltpu.VMEM((1, width), f32),
                pltpu.VMEM((nz, m, plane), bf),
                pltpu.VMEM((pairs, 2, plane, 2 * qf), bf),
                pltpu.VMEM((pairs, 2, plane, 2 * PF), bf),
                pltpu.VMEM((pairs, 2, plane, qf), bf),
                pltpu.VMEM((pairs, 2, plane, PF), bf),
                pltpu.VMEM((m, 2 * qf), f32),
                pltpu.VMEM((m, 2 * PF), f32),
                pltpu.VMEM((m, unit), bf),
                pltpu.VMEM((pairs, part, deep), f32),
                pltpu.VMEM((pairs, part, deep), bf),
                pltpu.VMEM((pairs, part, deep), bf),
                pltpu.VMEM((pairs, NX - 1, rows, deep), bf),
                pltpu.VMEM((pairs, NX - 1, rows, deep), bf),
                pltpu.VMEM((pairs, rows, deep), bf),
                dma((8,)),
                dma((pairs, 2)),
                dma((pairs + 1,)),
                dma((pairs + 1,)),
                dma((pairs + 1, NX - 1)),
                dma((pairs + 1, NX - 1)),
            ]
            + gather_sems * 2,
            compiler_params=pltpu.CompilerParams(collective_id=0, has_side_effects=True, vmem_limit_bytes=60 * 1024 * 1024),
        )(tokens, norm_gain.reshape(1, width), gate, up, down.T)

    return jax.shard_map(
        per_device,
        mesh=mesh,
        in_specs=(P("fs", None), P(), P("fs", "tp"), P("fs", "tp"), P("tp", "fs")),
        out_specs=P(("fs", "tp"), None),
        check_vma=False,
    )
```

time: 105 us -> 95.4 us (0.909)
  Pallas kernels: 103 us -> 93.5 us
    pallas_call x1, Pallas kernels: 103 us -> 93.5 us  [per_device(): pl.pallas_call(functools.partial(kernel, nz), out_shape=jax.ShapeDtypeStr...]
where the time goes in v2:
time: 95.4 us; the launch traced here: 95.2 us
  Pallas kernels  93.5 us (98%)
  local copies, waits for them, and re-layouts  1.77 us (2%)
    pallas_call x1, Pallas kernels, per_device(): pl.pallas_call(functools.partial(kernel, nz), out_shape=jax.ShapeDtypeStr...  93.5 us

profile of v2, /device:TPU:1, one launch (start us, length us, event | category | flops | bytes accessed | tf_op | source)
XLA Modules:
  0.0 95.2 jit_solution(13270990140871007632)
XLA Ops:
  0.0 93.5 %shard_map.55 = bf16[96,2048]{1,0:T(8,128)(2,1)} custom-call(bf16[768,2048]{1,0:T(8,128)(2,1)} %tok.1, f32[1,2048]{1,0:T(1,128)} %bitcast.3, bf16[32,640]{1,0:T(8,128)(2,1)} %gate.1, bf16[32,640]{1,0:T(8,128)(2,1)} %up.1, bf16[32,640]{1,0:T(8,128)(2,1)} %bitcast.2), custom_call_target="tpu_custom_call" | custom-call | tf_op jit(solution)/shard_map/pallas_call | solution.py:499
  93.5 1.8 %copy.7 = bf16[96,2048]{1,0:T(8,128)(2,1)} copy(bf16[96,2048]{1,0:T(8,128)(2,1)} %shard_map.55) | data formatting | bytes 786432
